TPU v7x, 512 devices: a whole 4x8x8 slice. The times are simulated.
512 devices in a mesh: sp: 32 (over z, x), tp: 16 (over y, core).
Axes of the slice: x: 4, y: 8, z: 8, core: 2. Of those that a mesh axis runs over, the one named last changes fastest.
Arguments:
- pool_input: bfloat16 [4096, 1024], P('sp', 'tp'), may hold values from -12 to 12
- doc_ids: int32 [4096], P('sp'), may hold values from 0 to 7, as said below
- residual: bfloat16 [4096, 2048], P('sp', 'tp'), may hold values from -30 to 30
- pool_gain: float32 [1024], P('tp'), may hold values from 0.1 to 1.9
- out_proj: bfloat16 [1024, 2048], P('tp'), may hold values from -0.25 to 0.25
- norm_gain: float32 [2048], P('tp'), may hold values from 0.1 to 1.9
- routes: int32 [4096, 2], P('sp'), may hold values from 0 to 31, all different within a row; in each aligned block of 128 rows (0 to 127, 128 to 255, ...) at most 16 rows name the same one
- route_weights: float32 [4096, 2], P('sp'), may hold values from 0.2 to 1.2
- expert_gate: bfloat16 [32, 2048, 4096], P('sp', None, 'tp'), may hold values from -0.125 to 0.125
- expert_up: bfloat16 [32, 2048, 4096], P('sp', None, 'tp'), may hold values from -0.125 to 0.125
- expert_down: bfloat16 [32, 4096, 2048], P('sp', 'tp'), may hold values from -0.125 to 0.125
- shared_gate: bfloat16 [2048, 1024], P(None, 'tp'), may hold values from -0.125 to 0.125
- shared_up: bfloat16 [2048, 1024], P(None, 'tp'), may hold values from -0.125 to 0.125
- shared_down: bfloat16 [1024, 2048], P('tp'), may hold values from -0.25 to 0.25
Outputs:
- layer_out: bfloat16 [4096, 2048], P('sp', 'tp')
Inputs may be any that keep to these rules, and one draw needn't show every extreme that they name: `routes`: each row names 2 different experts. In each aligned block of 128 rows no expert is named by more than 16 rows; in some blocks one expert is named by exactly 16 rows. `doc_ids`: document numbers start at 0, never fall along the sequence and rise by one at each document's start.
All inputs are finite; a program needn't handle non-finite values.
Results may differ from a plain program's by a relative error of at most 0.015.
Values may be sent and summed in bfloat16 or wider, within the bound.
A program may use at most 64 MiB of HBM per device.

v0:
```python
import jax
import jax.numpy as jnp
from jax import lax
from jax.sharding import PartitionSpec as P


def copy_for_each(value, axis):
    copies = jnp.broadcast_to(value, (lax.axis_size(axis), *value.shape))
    return lax.all_to_all(copies, axis, split_axis=0, concat_axis=0, tiled=True)


def gathered_once(value, axis):
    leaves = jax.tree.leaves(value)
    sequence = sorted(range(len(leaves)), key=lambda k: -leaves[k].size)
    width = (1, *leaves[sequence[0]].shape)[-1]
    lines = [
        jnp.pad(leaves[k].reshape(-1), (0, -leaves[k].size % width)).reshape(-1, width)
        for k in sequence
    ]
    both, at, found = (copy_for_each(jnp.concatenate(lines), axis), 0, {})
    for k, line in zip(sequence, lines):
        section = both[:, at : at + len(line)].reshape(len(both), -1)
        found[k] = section[:, : leaves[k].size].reshape(-1, *leaves[k].shape)
        at += len(line)
    numbers = iter(range(len(leaves)))
    return jax.tree.map(lambda _: found[next(numbers)], value)


def folded_in_pairs(pieces, combine):
    while len(jax.tree.leaves(pieces)[0]) > 1:
        pieces = jax.vmap(combine)(
            *(jax.tree.map(lambda part: part[side::2], pieces) for side in (0, 1))
        )
    return jax.tree.map(lambda part: part[0], pieces)


def carried_in(value, axis, combine, identity):
    size, position = (lax.axis_size(axis), lax.axis_index(axis))
    passed = jnp.arange(size) < position

    def kept(part, zero, own):
        part = jnp.where(
            passed.reshape(-1, *(1 for _ in own.shape)), part, jnp.asarray(zero, own.dtype)
        )
        return part

    pieces = gathered_once(value, axis)
    return folded_in_pairs(jax.tree.map(kept, pieces, identity, value), combine)


def from_behind(value, axis, by):
    size = lax.axis_size(axis)
    pairs = [(i, i + by) for i in range(size) if 0 <= i + by < size]
    return lax.ppermute(value, axis, pairs)


def split_up(value, dim, size):
    before, after = (value.shape[:dim], value.shape[dim + 1 :])
    return jnp.moveaxis(value.reshape(*before, size, -1, *after), dim, 0)


def sum_at_owner(value, axis, dim):
    blocks = split_up(value, dim, lax.axis_size(axis))
    arrived = lax.all_to_all(blocks, axis, split_axis=0, concat_axis=0, tiled=True)
    return arrived.astype(jnp.float32).sum(axis=0)


def over_copies(value, axis):
    return copy_for_each(value, axis).sum(axis=0)


def laid_out(blocks, dim):
    blocks = jnp.moveaxis(blocks, 0, dim)
    shape = blocks.shape
    return blocks.reshape(*shape[:dim], shape[dim] * shape[dim + 1], *shape[dim + 2 :])


def gathered_copies(value, axis, dim):
    blocks = copy_for_each(value, axis)
    return laid_out(blocks, dim)


def join_documents(earlier, later):
    earlier_sum, earlier_length, earlier_first, earlier_last, earlier_inner = earlier
    later_sum, later_length, later_first, later_last, later_inner = later
    boundary = later_first != earlier_last
    restart = (later_inner > 0) | boundary
    merged = (
        jnp.where(restart, later_sum, earlier_sum + later_sum),
        jnp.where(restart, later_length, earlier_length + later_length),
        earlier_first,
        later_last,
        jnp.maximum(jnp.maximum(earlier_inner, later_inner), boundary.astype(jnp.float32)),
    )
    earlier_empty = earlier_first < 0
    later_empty = later_first < 0
    return tuple(
        (
            jnp.where(earlier_empty, second, jnp.where(later_empty, first_value, joined))
            for first_value, second, joined in zip(earlier, later, merged)
        )
    )


def expert_terms(arrived, gate_weight, up_weight, down_weight):
    local_experts = gate_weight.shape[0]
    sources = arrived.shape[0] // local_experts
    grouped = arrived.reshape(sources, local_experts, arrived.shape[1], arrived.shape[2])
    gate = jnp.einsum("secd,edf->secf", grouped, gate_weight, preferred_element_type=jnp.float32)
    upper = jnp.einsum("secd,edf->secf", grouped, up_weight, preferred_element_type=jnp.float32)
    hidden = (jax.nn.silu(gate) * upper).astype(jnp.bfloat16)
    output = jnp.einsum("secf,efd->secd", hidden, down_weight, preferred_element_type=jnp.float32)
    return output.reshape(arrived.shape[0], arrived.shape[1], down_weight.shape[2])


def body(
    pool_input,
    doc_ids,
    residual,
    pool_gain,
    out_proj,
    norm_gain,
    routes,
    route_weights,
    expert_gate,
    expert_up,
    expert_down,
    shared_gate,
    shared_up,
    shared_down,
):
    row_count, channels = pool_input.shape
    values = pool_input.astype(jnp.float32)
    positions = jnp.arange(row_count, dtype=jnp.int32)
    inner_begin = jnp.concatenate([jnp.zeros((1,), bool), doc_ids[1:] != doc_ids[:-1]])
    running = jnp.cumsum(values[:, 3::4], axis=0)
    shifted = jnp.concatenate([jnp.zeros((1, running.shape[1]), jnp.float32), running], 0)
    inner_last = jnp.max(jnp.where(inner_begin, positions, 0))
    own_terms = (
        running[-1] - shifted[inner_last],
        (row_count - inner_last).astype(jnp.float32),
        doc_ids[0].astype(jnp.float32),
        doc_ids[-1].astype(jnp.float32),
        jnp.any(inner_begin).astype(jnp.float32),
    )
    identity = (
        jnp.zeros((running.shape[1],), jnp.float32),
        jnp.zeros((), jnp.float32),
        jnp.full((), -1.0, jnp.float32),
        jnp.full((), -1.0, jnp.float32),
        jnp.zeros((), jnp.float32),
    )
    before = carried_in(own_terms, "sp", join_documents, identity)
    fresh = (before[2] < 0) | (doc_ids[0].astype(jnp.float32) != before[3])
    begins = jnp.concatenate([fresh[None], inner_begin[1:]])
    doc_start = lax.cummax(jnp.where(begins, positions, -1), axis=0)
    found = doc_start >= 0
    carry_sum = jnp.where(fresh, 0.0, before[0])
    carry_length = jnp.where(fresh, 0.0, before[1])
    length = jnp.where(
        found,
        (positions - doc_start + 1).astype(jnp.float32),
        carry_length + (positions + 1).astype(jnp.float32),
    )
    start_rows = jnp.take(shifted, jnp.maximum(doc_start, 0), axis=0)
    doc_sum = jnp.where(found[:, None], running - start_rows, carry_sum[None, :] + running)
    doc_mean = doc_sum / length[:, None]
    rim = from_behind(pool_input[row_count - 15 :], "sp", 1)
    extended = jnp.concatenate([rim, pool_input], 0).astype(jnp.float32)
    scale_index = jnp.arange(channels, dtype=jnp.int32) % 4
    window_size = jnp.where(scale_index == 0, 2.0, jnp.where(scale_index == 1, 8.0, 16.0))
    window_total = jnp.zeros((row_count, channels), jnp.float32)
    for offset in range(16):
        inside = (offset < length[:, None]) & (offset < window_size[None, :])
        window_total = window_total + jnp.where(
            inside, extended[15 - offset : 15 - offset + row_count], 0.0
        )
    window_mean = window_total / jnp.minimum(length[:, None], window_size[None, :])
    pool_mean = jnp.concatenate(
        [window_mean.reshape(row_count, channels // 4, 4)[..., :3], doc_mean[..., None]], -1
    )
    pool_mean = pool_mean.reshape(row_count, channels)
    pooled = ((pool_mean - values) * pool_gain).astype(jnp.bfloat16)
    terms = jnp.dot(pooled, out_proj, preferred_element_type=jnp.float32)
    projected = sum_at_owner(terms.astype(jnp.bfloat16), "tp", 1).astype(jnp.bfloat16)
    hidden_state = residual.astype(jnp.float32) + projected.astype(jnp.float32)
    squares = over_copies(jnp.sum(hidden_state * hidden_state, axis=1), "tp")
    model_width = residual.shape[1] * lax.axis_size("tp")
    scaling = lax.rsqrt(squares / model_width + 1e-06)
    normed_columns = (hidden_state * scaling[:, None] * norm_gain).astype(jnp.bfloat16)
    normed = gathered_copies(normed_columns, "tp", 1)
    shared_gate_out = jnp.dot(normed, shared_gate, preferred_element_type=jnp.float32)
    shared_up_out = jnp.dot(normed, shared_up, preferred_element_type=jnp.float32)
    shared_hidden = (jax.nn.silu(shared_gate_out) * shared_up_out).astype(jnp.bfloat16)
    shared_terms = jnp.dot(shared_hidden, shared_down, preferred_element_type=jnp.float32)
    group_size = lax.axis_size("tp")
    experts = expert_gate.shape[0] * lax.axis_size("sp")
    top = routes.shape[1]
    capacity = group_size * max(1, 2 * row_count * top // (experts * group_size))
    flat_experts = routes.reshape(-1)
    onehot = (flat_experts[:, None] == jnp.arange(experts, dtype=jnp.int32)[None, :]).astype(
        jnp.int32
    )
    ranks = jnp.sum((jnp.cumsum(onehot, axis=0) - 1) * onehot, axis=1)
    slots = flat_experts * capacity + ranks
    token_index = jnp.arange(row_count * top, dtype=jnp.int32) // top
    slot_token = jnp.full((experts * capacity,), row_count, jnp.int32).at[slots].set(token_index)
    with_blank = jnp.concatenate([normed, jnp.zeros((1, normed.shape[1]), jnp.bfloat16)], 0)
    outgoing = jnp.take(with_blank, slot_token, axis=0).reshape(experts, capacity, normed.shape[1])
    expert_parts = expert_terms(
        lax.all_to_all(outgoing, "sp", split_axis=0, concat_axis=0, tiled=True),
        expert_gate,
        expert_up,
        expert_down,
    )
    routed_sum, shared_sum = (
        sum_at_owner(expert_parts.astype(jnp.bfloat16), "tp", 2),
        sum_at_owner(shared_terms[None].astype(jnp.bfloat16), "tp", 2),
    )
    returned = lax.all_to_all(
        routed_sum.astype(jnp.bfloat16), "sp", split_axis=0, concat_axis=0, tiled=True
    )
    flat_back = returned.reshape(experts * capacity, returned.shape[2])
    picked = (
        jnp.take(flat_back, slots, axis=0).astype(jnp.float32) * route_weights.reshape(-1)[:, None]
    )
    routed = jnp.sum(picked.reshape(row_count, top, flat_back.shape[1]), axis=1)
    shared_out = shared_sum[0].astype(jnp.bfloat16).astype(jnp.float32)
    return (hidden_state + routed + shared_out).astype(jnp.bfloat16)


def solution(mesh):
    placed = (
        P("sp", "tp"),
        P("sp"),
        P("sp", "tp"),
        P("tp"),
        P("tp", None),
        P("tp"),
        P("sp", None),
        P("sp", None),
        P("sp", None, "tp"),
        P("sp", None, "tp"),
        P("sp", "tp", None),
        P(None, "tp"),
        P(None, "tp"),
        P("tp", None),
    )
    return jax.shard_map(body, mesh=mesh, in_specs=placed, out_specs=P("sp", "tp"), check_vma=False)
```

profile of v0, /device:TPU:1, one launch (start us, length us, event | category | flops | bytes accessed | tf_op | source)
XLA Modules:
  0.0 278.8 jit_solution(7757600359169477122)
XLA Ops:
  0.0 1.5 fusion.75
  1.5 1.3 fusion.80
  2.8 0.7 slice.262
  3.6 0.8 fusion.66
  7.7 0.7 fusion.65
  8.4 0.2 reduce_window_sum.26
  9.3 0.6 broadcast_in_dim.215
  9.9 13.7 %all-to-all-start = ((f32[32,5,16]{2,1,0:T(8,128)}), f32[32,5,16]{2,1,0:T(8,128)S(1)}, u32[]{:S(2)}, u32[]{:S(2)}) async-start(f32[32,5,16]{2,1,0:T(8,128)} %broadcast_in_dim.215), calls=%async_computation | async-start | bytes 262144 | tf_op jit(solution)/shard_map/all_to_all | solution.py:9
  23.7 0.8 slice.315
  24.5 3.1 %collective-permute-start = (bf16[15,64]{0,1:T(8,128)(2,1)S(1)}, bf16[15,64]{0,1:T(8,128)(2,1)S(1)}, u32[]{:S(2)}, u32[]{:S(2)}) collective-permute-start(bf16[15,64]{0,1:T(8,128)(2,1)S(1)} %slice.315), channel_id=1, source_target_pairs={{0,16},{16,32},{32,48},{48,64},{64,80},{80,96},{96,112},{112,128},... | collective-permute-start | bytes 5768 | tf_op jit(solution)/shard_map/ppermute | solution.py:54
  27.8 0.6 collective-permute-done
  28.4 0.8 maximum_convert_fusion
  29.2 3.8 %all-to-all-done = f32[32,5,16]{2,1,0:T(8,128)S(1)} async-done(((f32[32,5,16]{2,1,0:T(8,128)}), f32[32,5,16]{2,1,0:T(8,128)S(1)}, u32[]{:S(2)}, u32[]{:S(2)}) %all-to-all-start) | async-done | bytes 10272 | tf_op jit(solution)/shard_map/all_to_all | solution.py:9
  37.3 0.6 fusion.79
  40.5 0.6 fusion.78
  44.4 0.1 copy.66
  44.5 0.2 reduce-window.10
  44.8 0.6 gather_fusion
  45.5 0.7 fusion.77
  46.2 0.6 slice.314
  50.8 0.3 fusion.19
  51.2 0.4 fusion
  51.6 0.9 copy.96
  52.5 9.2 %all-to-all-start.1 = ((bf16[16,128,128]{2,1,0:T(8,128)(2,1)}), bf16[16,128,128]{2,1,0:T(8,128)(2,1)S(1)}, u32[]{:S(2)}, u32[]{:S(2)}) async-start(bf16[16,128,128]{2,1,0:T(8,128)(2,1)} %bitcast.147), calls=%async_computation.1 | async-start | bytes 1048576 | tf_op jit(solution)/shard_map/all_to_all | solution.py:64
  61.7 0.1 copy.71
  61.8 0.1 eq.209
  62.0 0.6 reduce-window.11
  62.6 16.3 %all-to-all-done.1 = bf16[16,128,128]{2,1,0:T(8,128)(2,1)S(1)} async-done(((bf16[16,128,128]{2,1,0:T(8,128)(2,1)}), bf16[16,128,128]{2,1,0:T(8,128)(2,1)S(1)}, u32[]{:S(2)}, u32[]{:S(2)}) %all-to-all-start.1) | async-done | bytes 524320 | tf_op jit(solution)/shard_map/all_to_all | solution.py:64
  79.1 0.6 broadcast_in_dim.248
  79.7 3.4 %all-to-all-start.2 = ((f32[16,1,128]{2,1,0:T(1,128)}), f32[16,1,128]{2,1,0:T(1,128)S(1)}, u32[]{:S(2)}, u32[]{:S(2)}) async-start(f32[16,1,128]{2,1,0:T(1,128)} %broadcast_in_dim.248), calls=%async_computation.2 | async-start | bytes 16384 | tf_op jit(solution)/shard_map/all_to_all | solution.py:9
  83.1 0.2 slice_reduce_fusion
  83.3 0.1 reshape.565
  83.4 0.1 copy.76
  83.5 0.1 mul.77
  83.7 6.0 %all-to-all-done.2 = f32[16,1,128]{2,1,0:T(1,128)S(1)} async-done(((f32[16,1,128]{2,1,0:T(1,128)}), f32[16,1,128]{2,1,0:T(1,128)S(1)}, u32[]{:S(2)}, u32[]{:S(2)}) %all-to-all-start.2) | async-done | bytes 8224 | tf_op jit(solution)/shard_map/all_to_all | solution.py:9
  89.8 0.9 broadcast_in_dim.249
  90.7 4.0 %all-to-all-start.3 = ((bf16[16,128,128]{2,1,0:T(8,128)(2,1)}), bf16[16,128,128]{2,1,0:T(8,128)(2,1)S(1)}, u32[]{:S(2)}, u32[]{:S(2)}) async-start(bf16[16,128,128]{2,1,0:T(8,128)(2,1)} %broadcast_in_dim.249), calls=%async_computation.3 | async-start | bytes 1048576 | tf_op jit(solution)/shard_map/all_to_all | solution.py:9
  94.8 1.4 scatter_custom_fusion
  96.3 15.7 %all-to-all-done.3 = bf16[16,128,128]{2,1,0:T(8,128)(2,1)S(1)} async-done(((bf16[16,128,128]{2,1,0:T(8,128)(2,1)}), bf16[16,128,128]{2,1,0:T(8,128)(2,1)S(1)}, u32[]{:S(2)}, u32[]{:S(2)}) %all-to-all-start.3) | async-done | bytes 524320 | tf_op jit(solution)/shard_map/all_to_all | solution.py:9
  112.0 0.8 copy-done.1
  112.9 3.3 %gather_fusion.1 = bf16[512,2048]{1,0:T(8,128)(2,1)} fusion(bf16[129,2048]{1,0:T(8,128)(2,1)S(1)} %concatenate.40, s32[1024]{0:T(1024)S(1)} %pad_clamp_fusion.1), kind=kCustom, calls=%fused_computation.1 | custom fusion | bytes 4196352 | tf_op jit(solution)/shard_map/jit(_take)/gather | solution.py:209
  116.3 1.8 broadcast_select_fusion
  118.1 57.3 %all_to_all.41 = bf16[32,16,2048]{2,1,0:T(8,128)(2,1)S(1)} all-to-all(bf16[32,16,2048]{2,1,0:T(8,128)(2,1)S(1)} %broadcast_select_fusion), channel_id=1, replica_groups=mesh['sp'=32,'tp'=16] {'sp'}, dimensions={0} | all-to-all | bytes 4194304 | tf_op jit(solution)/shard_map/all_to_all | solution.py:211
  175.4 1.5 convolution_bitcast_fusion.1
  176.9 5.0 %convolution_convert_fusion = bf16[32,16,2048]{2,1,0:T(8,128)(2,1)} fusion(bf16[32,16,2048]{2,1,0:T(8,128)(2,1)S(1)} %all_to_all.41, bf16[1,256,2048]{2,1,0:T(8,128)(2,1)S(1)} %copy-done, bf16[1,2048,256]{2,1,0:T(8,128)(2,1)} %param.23, f32[32,1,16,256]{3,2,0,1:T(8,128)} %convolution_bitcast_fusion.1), kind=kOutput, calls=%fused_computation.4 | convolution fusion | flops 1075576832 | bytes 6815744 | tf_op jit(solution)/shard_map/secf,efd->secd/dot_general | solution.py:112
  181.9 2.2 copy.85
  184.2 1.9 copy.95
  186.1 4.0 %all-to-all-start.5 = ((bf16[16,32,16,128]{3,2,1,0:T(8,128)(2,1)}), bf16[16,32,16,128]{3,2,1,0:T(8,128)(2,1)S(1)}, u32[]{:S(2)}, u32[]{:S(2)}) async-start(bf16[16,32,16,128]{3,2,1,0:T(8,128)(2,1)} %bitcast.151), calls=%async_computation.5 | async-start | bytes 4194304 | tf_op jit(solution)/shard_map/all_to_all | solution.py:64
  190.1 1.4 fusion.73
  191.5 2.8 fusion.1
  194.3 1.1 copy.86
  195.4 0.9 copy.97
  196.4 42.8 %all-to-all-done.5 = bf16[16,32,16,128]{3,2,1,0:T(8,128)(2,1)S(1)} async-done(((bf16[16,32,16,128]{3,2,1,0:T(8,128)(2,1)}), bf16[16,32,16,128]{3,2,1,0:T(8,128)(2,1)S(1)}, u32[]{:S(2)}, u32[]{:S(2)}) %all-to-all-start.5) | async-done | bytes 2097184 | tf_op jit(solution)/shard_map/all_to_all | solution.py:64
  239.2 4.8 %all-to-all-start.7 = ((bf16[16,1,128,128]{3,2,1,0:T(8,128)(2,1)}), bf16[16,1,128,128]{3,2,1,0:T(8,128)(2,1)}, u32[]{:S(2)}, u32[]{:S(2)}) async-start(bf16[16,1,128,128]{3,2,1,0:T(8,128)(2,1)} %bitcast.155), calls=%async_computation.7 | async-start | bytes 1048576 | tf_op jit(solution)/shard_map/all_to_all | solution.py:64
  244.0 0.1 reduce_sum.78
  244.2 1.0 reduce_sum.82
  245.2 16.1 %all-to-all-done.7 = bf16[16,1,128,128]{3,2,1,0:T(8,128)(2,1)} async-done(((bf16[16,1,128,128]{3,2,1,0:T(8,128)(2,1)}), bf16[16,1,128,128]{3,2,1,0:T(8,128)(2,1)}, u32[]{:S(2)}, u32[]{:S(2)}) %all-to-all-start.7) | async-done | bytes 524320 | tf_op jit(solution)/shard_map/all_to_all | solution.py:64
  261.4 5.2 %all-to-all-start.6 = ((bf16[32,16,128]{2,1,0:T(8,128)(2,1)}), bf16[32,16,128]{2,1,0:T(8,128)(2,1)S(1)}, u32[]{:S(2)}, u32[]{:S(2)}) async-start(bf16[32,16,128]{2,1,0:T(8,128)(2,1)} %reduce_sum.82), calls=%async_computation.6 | async-start | bytes 262144 | tf_op jit(solution)/shard_map/all_to_all | solution.py:220
  266.6 0.1 copy.75
  266.8 1.1 reduce_sum.84
  267.9 9.0 %all-to-all-done.6 = bf16[32,16,128]{2,1,0:T(8,128)(2,1)S(1)} async-done(((bf16[32,16,128]{2,1,0:T(8,128)(2,1)}), bf16[32,16,128]{2,1,0:T(8,128)(2,1)S(1)}, u32[]{:S(2)}, u32[]{:S(2)}) %all-to-all-start.6) | async-done | bytes 131104 | tf_op jit(solution)/shard_map/all_to_all | solution.py:220
  276.9 0.9 gather_fusion.2
  277.8 0.3 multiply_reduce_fusion
  278.1 0.6 add_convert_fusion
  (135 shorter events, 5.8 us)
Async XLA Ops:
  0.0 176.9 %copy-start = (bf16[1,256,2048]{2,1,0:T(8,128)(2,1)S(1)}, bf16[1,256,2048]{2,1,0:T(8,128)(2,1)}, u32[]{:S(2)}) copy-start(bf16[1,256,2048]{2,1,0:T(8,128)(2,1)} %param.24) | copy-start | bytes 3145732
  0.0 51.2 %copy-start.5 = (bf16[128,64]{0,1:T(8,128)(2,1)S(1)}, bf16[128,64]{0,1:T(8,128)(2,1)}, u32[]{:S(2)}) copy-start(bf16[128,64]{0,1:T(8,128)(2,1)} %param.14) | copy-start | bytes 49156
  0.0 51.2 %copy-start.3 = (bf16[64,2048]{1,0:T(8,128)(2,1)S(1)}, bf16[64,2048]{1,0:T(8,128)(2,1)}, u32[]{:S(2)}) copy-start(bf16[64,2048]{1,0:T(8,128)(2,1)} %param.18) | copy-start | bytes 786436
  0.0 51.2 %copy-start.9 = (f32[64]{0:T(128)S(1)}, f32[64]{0:T(128)}, u32[]{:S(2)}) copy-start(f32[64]{0:T(128)} %param.17) | copy-start | bytes 772
  9.9 23.1 %all-to-all-start = ((f32[32,5,16]{2,1,0:T(8,128)}), f32[32,5,16]{2,1,0:T(8,128)S(1)}, u32[]{:S(2)}, u32[]{:S(2)}) async-start(f32[32,5,16]{2,1,0:T(8,128)} %broadcast_in_dim.215), calls=%async_computation | async-start | bytes 262144 | tf_op jit(solution)/shard_map/all_to_all | solution.py:9
  24.5 4.0 %collective-permute-start = (bf16[15,64]{0,1:T(8,128)(2,1)S(1)}, bf16[15,64]{0,1:T(8,128)(2,1)S(1)}, u32[]{:S(2)}, u32[]{:S(2)}) collective-permute-start(bf16[15,64]{0,1:T(8,128)(2,1)S(1)} %slice.315), channel_id=1, source_target_pairs={{0,16},{16,32},{32,48},{48,64},{64,80},{80,96},{96,112},{112,128},... | collective-permute-start | bytes 5768 | tf_op jit(solution)/shard_map/ppermute | solution.py:54
  44.8 16.9 %copy-start.6 = (s32[128,2]{0,1:T(2,128)S(1)}, s32[128,2]{0,1:T(2,128)}, u32[]{:S(2)}) copy-start(s32[128,2]{0,1:T(2,128)} %param.20) | copy-start | bytes 3076
  50.8 28.2 %copy-start.2 = (bf16[128,128]{1,0:T(8,128)(2,1)S(1)}, bf16[128,128]{1,0:T(8,128)(2,1)}, u32[]{:S(2)}) copy-start(bf16[128,128]{1,0:T(8,128)(2,1)} %param.16) | copy-start | bytes 98308
  51.1 38.6 %copy-start.8 = (f32[128]{0:T(128)S(1)}, f32[128]{0:T(128)}, u32[]{:S(2)}) copy-start(f32[128]{0:T(128)} %param.19) | copy-start | bytes 1540
  52.5 26.4 %all-to-all-start.1 = ((bf16[16,128,128]{2,1,0:T(8,128)(2,1)}), bf16[16,128,128]{2,1,0:T(8,128)(2,1)S(1)}, u32[]{:S(2)}, u32[]{:S(2)}) async-start(bf16[16,128,128]{2,1,0:T(8,128)(2,1)} %bitcast.147), calls=%async_computation.1 | async-start | bytes 1048576 | tf_op jit(solution)/shard_map/all_to_all | solution.py:64
  79.7 10.0 %all-to-all-start.2 = ((f32[16,1,128]{2,1,0:T(1,128)}), f32[16,1,128]{2,1,0:T(1,128)S(1)}, u32[]{:S(2)}, u32[]{:S(2)}) async-start(f32[16,1,128]{2,1,0:T(1,128)} %broadcast_in_dim.248), calls=%async_computation.2 | async-start | bytes 16384 | tf_op jit(solution)/shard_map/all_to_all | solution.py:9
  90.7 21.3 %all-to-all-start.3 = ((bf16[16,128,128]{2,1,0:T(8,128)(2,1)}), bf16[16,128,128]{2,1,0:T(8,128)(2,1)S(1)}, u32[]{:S(2)}, u32[]{:S(2)}) async-start(bf16[16,128,128]{2,1,0:T(8,128)(2,1)} %broadcast_in_dim.249), calls=%async_computation.3 | async-start | bytes 1048576 | tf_op jit(solution)/shard_map/all_to_all | solution.py:9
  112.0 0.8 copy-start.1
  118.1 57.3 %copy-start.10 = (bf16[1,2048,256]{2,1,0:T(8,128)(2,1)S(1)}, bf16[1,2048,256]{2,1,0:T(8,128)(2,1)}, u32[]{:S(2)}) copy-start(bf16[1,2048,256]{2,1,0:T(8,128)(2,1)} %param.22) | copy-start | bytes 3145732
  186.1 5.4 %copy-start.4 = (bf16[64,2048]{1,0:T(8,128)(2,1)S(1)}, bf16[64,2048]{1,0:T(8,128)(2,1)}, u32[]{:S(2)}) copy-start(bf16[64,2048]{1,0:T(8,128)(2,1)} %param.27) | copy-start | bytes 786436
  186.1 53.1 %all-to-all-start.5 = ((bf16[16,32,16,128]{3,2,1,0:T(8,128)(2,1)}), bf16[16,32,16,128]{3,2,1,0:T(8,128)(2,1)S(1)}, u32[]{:S(2)}, u32[]{:S(2)}) async-start(bf16[16,32,16,128]{3,2,1,0:T(8,128)(2,1)} %bitcast.151), calls=%async_computation.5 | async-start | bytes 4194304 | tf_op jit(solution)/shard_map/all_to_all | solution.py:64
  196.4 70.3 %copy-start.7 = (f32[128,2]{0,1:T(2,128)S(1)}, f32[128,2]{0,1:T(2,128)}, u32[]{:S(2)}) copy-start(f32[128,2]{0,1:T(2,128)} %param.21) | copy-start | bytes 3076
  239.2 22.1 %all-to-all-start.7 = ((bf16[16,1,128,128]{3,2,1,0:T(8,128)(2,1)}), bf16[16,1,128,128]{3,2,1,0:T(8,128)(2,1)}, u32[]{:S(2)}, u32[]{:S(2)}) async-start(bf16[16,1,128,128]{3,2,1,0:T(8,128)(2,1)} %bitcast.155), calls=%async_computation.7 | async-start | bytes 1048576 | tf_op jit(solution)/shard_map/all_to_all | solution.py:64
  261.4 15.6 %all-to-all-start.6 = ((bf16[32,16,128]{2,1,0:T(8,128)(2,1)}), bf16[32,16,128]{2,1,0:T(8,128)(2,1)S(1)}, u32[]{:S(2)}, u32[]{:S(2)}) async-start(bf16[32,16,128]{2,1,0:T(8,128)(2,1)} %reduce_sum.82), calls=%async_computation.6 | async-start | bytes 262144 | tf_op jit(solution)/shard_map/all_to_all | solution.py:220
where the time goes:
time: 280 us; the launch traced here: 279 us
  waiting for transfers between devices  110 us (39%)
  blocking collectives  57.3 us (20%)
  starting transfers between devices  47.4 us (17%)
  local copies, waits for them, and re-layouts  27.3 us (10%)
  between operations  14 us (5%)
  other arithmetic  11.3 us (4%)
  matrix products  11.1 us (4%)
    all_to_all x3, waiting for transfers between devices, sum_at_owner(): lax.all_to_all(blocks, axis, split_axis=0, concat_axis=0, tiled=True)  75.3 us
    all_to_all x1, blocking collectives, body(): lax.all_to_all(outgoing, 'sp', split_axis=0, concat_axis=0, tiled=True)  57.3 us
    all_to_all x3, waiting for transfers between devices, copy_for_each(): return lax.all_to_all(copies, axis, split_axis=0, concat_axis=0, tiled=True)  25.4 us
    all_to_all x3, starting transfers between devices, copy_for_each(): return lax.all_to_all(copies, axis, split_axis=0, concat_axis=0, tiled=True)  21.1 us
    all_to_all x3, starting transfers between devices, sum_at_owner(): lax.all_to_all(blocks, axis, split_axis=0, concat_axis=0, tiled=True)  18 us
    all_to_all x1, waiting for transfers between devices, body(): lax.all_to_all(routed_sum.astype(jnp.bfloat16), 'sp', split_axis=0, conca...  8.96 us
    slice x44, local copies, waits for them, and re-layouts, folded_in_pairs(): part[side::2]  5.8 us
  transfers between devices with their start and end apart: 8, of which 8 were waited for; matrix products, arithmetic and copies ran while one was open for 5% of the time, Pallas kernels for 0%

commit v1 on v0

v1 whole, which is shorter than its diff:
```python
import functools

import jax
import jax.numpy as jnp
from jax import lax
from jax.experimental import pallas as pl
from jax.experimental.pallas import tpu as pltpu
from jax.sharding import PartitionSpec as P

MESH = pl.DeviceIdType.MESH
F32 = jnp.float32
BF16 = jnp.bfloat16
VMEM = pltpu.VMEM
DMA = pltpu.SemaphoreType.DMA


def dot(a, b):
    return jnp.dot(a, b, preferred_element_type=F32)


def dot_nt(a, b):
    return lax.dot_general(a, b, (((1,), (1,)), ((), ())), preferred_element_type=F32)


def dot_tn(a, b):
    return lax.dot_general(a, b, (((0,), (0,)), ((), ())), preferred_element_type=F32)


def silu(v):
    return v * (1.0 / (1.0 + jnp.exp(-v)))


def iota(shape, dim):
    return lax.broadcasted_iota(jnp.int32, shape, dim)


def ones_where(mask):
    return jnp.where(mask, 1.0, 0.0)


def as_columns(row, size):
    return jnp.transpose(jnp.broadcast_to(row, (size, size)))


def kernel(
    cfg,
    xt_ref, ids_ref, residual_ref, pgain_ref, ngain_ref, routes_ref, weights_ref,
    oproj_hbm, eg_hbm, eu_hbm, ed_hbm, sg_hbm, su_hbm, sd_hbm,
    out_ref,
    oproj, eg, eu, ed, sgu, sd, local_sem,
    cb, xprev, wq, gn, pk, dsp, big, part, qbuf, ra, rb, sa, sb, fin, back,
    gbuf, hbuf, accg, accu, ssq, accs, sss, slot_scr,
    send, carry_sem, rim_sem, wq_sem, gn_sem, pk_sem, disp_sem, ring_a, ring_b,
    peer_sem, q_sem, rs_a, rs_b, back_sem,
):
    NS, NT, T, CAP, NCH = cfg
    Y = NT // 2
    R = NS * CAP
    RC = R // NCH
    BPC = NS // NCH
    NA, NB = Y // 2, Y - 1 - Y // 2
    D = NT * T
    s = lax.axis_index("sp")
    me = lax.axis_index("tp")
    y = me // 2
    c = me % 2
    partner = (s, y * 2 + 1 - c)
    sign = 1 - 2 * c

    def chip(off):
        return lax.rem(y + off + 2 * Y, Y)

    def rcopy(src, dst, ssem, rsem, dev):
        return pltpu.make_async_remote_copy(
            src_ref=src, dst_ref=dst, send_sem=ssem, recv_sem=rsem, device_id=dev, device_id_type=MESH
        )

    def arrived(ref, rsem):
        rcopy(ref, ref, send.at[0], rsem, partner).wait_recv()

    def sent(ref, k):
        rcopy(ref, ref, send.at[k], rim_sem.at[0], partner).wait_send()

    loads = [
        pltpu.make_async_copy(src, dst, local_sem.at[k])
        for k, (src, dst) in enumerate(
            [
                (oproj_hbm, oproj),
                (eg_hbm.at[0], eg),
                (eu_hbm.at[0], eu),
                (ed_hbm.at[0], ed),
                (sg_hbm, sgu.at[pl.ds(0, 64)]),
                (su_hbm, sgu.at[pl.ds(64, 64)]),
                (sd_hbm, sd),
            ]
        )
    ]
    for load in loads:
        load.start()

    barrier = pltpu.get_barrier_semaphore()

    def greet_sp(k, _):
        pl.semaphore_signal(barrier, inc=1, device_id=(lax.rem(s + k, NS), me), device_id_type=MESH)
        return 0

    def greet_tp(k, _):
        pl.semaphore_signal(barrier, inc=1, device_id=(s, lax.rem(me + k, NT)), device_id_type=MESH)
        return 0

    lax.fori_loop(1, NS, greet_sp, 0)
    lax.fori_loop(1, NT, greet_tp, 0)

    xt = xt_ref[...]
    ids = ids_ref[...].astype(F32)
    lane1 = iota((1, T), 1)
    d0 = jnp.sum(jnp.where(lane1 == 0, ids, 0.0), axis=1, keepdims=True)
    d_last = jnp.sum(jnp.where(lane1 == T - 1, ids, 0.0), axis=1, keepdims=True)
    tail = ones_where(ids == d_last)
    tail_len = jnp.sum(tail, axis=1, keepdims=True)
    tail_sum = dot_nt(jnp.broadcast_to(tail, (8, T)).astype(BF16), xt)[0:1, :]
    cb[pl.ds(s, 1), :, :] = jnp.where(
        lane1 == 0, tail_len, jnp.where(lane1 == 1, d_last, 0.0)
    ).reshape(1, 1, T)
    cb[pl.ds(s, 1), :, 64:128] = tail_sum.reshape(1, 1, 64)
    gn[pl.ds(me, 1), :, :] = ngain_ref[...].reshape(1, 1, T)

    loads[0].wait()
    pl.semaphore_wait(barrier, NS - 1 + NT - 1)

    def send_carry(k, _):
        to = (lax.rem(s + k, NS), me)
        rcopy(cb.at[s], cb.at[s], send.at[0], carry_sem.at[0], to).start()
        return 0

    lax.fori_loop(1, NS, send_carry, 0)
    rcopy(xt_ref, xprev, send.at[3], rim_sem.at[0], (lax.rem(s + 1, NS), me)).start()

    def send_proj(k, _):
        j = lax.rem(me + k, NT)
        to = (s, j)
        cols = oproj.at[:, pl.ds(pl.multiple_of(j * T, T), T)]
        rcopy(cols, wq.at[me], send.at[1], wq_sem.at[0], to).start()
        rcopy(gn.at[me], gn.at[me], send.at[2], gn_sem.at[0], to).start()
        return 0

    lax.fori_loop(1, NT, send_proj, 0)
    wq[pl.ds(me, 1), :, :] = oproj[:, pl.ds(pl.multiple_of(me * T, T), T)].reshape(1, 64, T)

    su_i, la_i = iota((T, T), 0), iota((T, T), 1)
    ids_t = jnp.broadcast_to(ids, (T, T))
    causal = (jnp.transpose(ids_t) == ids_t) & (su_i <= la_i)
    windows = (2, 8, 16)
    scale = lax.rem(iota((64, T), 0), 4)

    def by_scale(a0, a1, a2, a3):
        return jnp.where(scale == 0, a0, jnp.where(scale == 1, a1, jnp.where(scale == 2, a2, a3)))

    own = [dot(xt, ones_where(causal & (la_i - su_i < w)).astype(BF16)) for w in windows]
    all_own = ones_where(causal)
    total = by_scale(*own, dot(xt, all_own.astype(BF16)))
    count = jnp.sum(all_own, axis=0, keepdims=True)
    gbuf[...] = jnp.zeros_like(gbuf)
    gbuf[:, 0:64] = pgain_ref[...]
    gain_t = as_columns(gbuf[...], T)[0:64, :]

    experts = routes_ref[...]
    hits = [ones_where(iota((T, T), 0) == experts[k : k + 1, :]) for k in range(2)]
    earlier = dot((hits[0] + hits[1]).astype(BF16), ones_where(su_i < la_i).astype(BF16))
    slots = [
        experts[k : k + 1, :].astype(F32) * CAP
        + jnp.sum(earlier * hits[k], axis=0, keepdims=True)
        for k in range(2)
    ]
    for k in range(2):
        slot_scr[k : k + 1, :] = slots[k]

    arrived(cb.at[pl.ds(0, NS - 1)], carry_sem.at[0])
    tails = cb[...]
    lane3 = iota((NS, 1, T), 2)
    last_ids = jnp.sum(jnp.where(lane3 == 1, tails, 0.0), axis=2, keepdims=True)
    used = (iota((NS, 1, T), 0) < s) & (last_ids == d0.reshape(1, 1, 1))
    carried = jnp.sum(jnp.where(used, tails, 0.0), axis=0)
    carry_len = jnp.sum(jnp.where(lane1 == 0, carried, 0.0), axis=1, keepdims=True)
    carry_t = as_columns(carried, T)[64:128, :]
    first_doc = ids == d0
    length = count + jnp.where(first_doc, carry_len, 0.0)
    arrived(xprev, rim_sem.at[0])
    before = (su_i.astype(F32) >= T - carry_len) & first_doc
    prev = xprev[...]
    past = [dot(prev, ones_where(before & (la_i + T - su_i < w)).astype(BF16)) for w in windows]
    total = total + by_scale(*past, jnp.where(first_doc, carry_t, 0.0))
    spans = [jnp.broadcast_to(jnp.minimum(length, float(w)), (64, T)) for w in windows]
    mean = total / by_scale(*spans, jnp.broadcast_to(length, (64, T)))
    pooled = ((mean - xt.astype(F32)) * gain_t).astype(BF16)
    pk[pl.ds(me, 1), :, :] = pooled.reshape(1, 64, T)

    def give_partner(j):
        rcopy(pk.at[j], pk.at[j], send.at[4], pk_sem.at[j], partner).start()

    far_first = sorted([o for o in range(1, Y)], key=lambda o: -min(o, Y - o))
    for off in far_first:
        to = (s, chip(off) * 2 + c)
        rcopy(pk.at[me], pk.at[me], send.at[4], pk_sem.at[me], to).start()
    give_partner(me)
    for off in reversed(far_first):
        j = chip(off) * 2 + c
        arrived(pk.at[j], pk_sem.at[j])
        give_partner(j)
    arrived(wq.at[pl.ds(0, NT - 1)], wq_sem.at[0])
    for off in [0] + list(reversed(far_first)):
        j = chip(off) * 2 + 1 - c
        arrived(pk.at[j], pk_sem.at[j])
    projected = dot_tn(pk[...].reshape(NT * 64, T), wq[...].reshape(NT * 64, T)).astype(BF16)
    hidden_state = residual_ref[...].astype(F32) + projected.astype(F32)
    hbuf[...] = hidden_state
    rows = hidden_state.astype(BF16)
    big[pl.ds(me, 1), 0:T, :] = rows.reshape(1, T, T)

    srow = iota((R, T), 0).astype(F32)
    chosen = ones_where((srow == slot_scr[0:1, :]) | (srow == slot_scr[1:2, :])).astype(BF16)
    dsp[...] = dot(chosen, rows).astype(BF16)

    def block_rows(ref, b, base=0):
        return ref.at[pl.ds(pl.multiple_of(base + b * CAP, 16), CAP)]

    def send_rows(k, _):
        b = lax.rem(s + k, NS)
        rcopy(
            block_rows(dsp, b), block_rows(big.at[me], s, T), send.at[5], disp_sem.at[s], (b, me)
        ).start()
        return 0

    lax.fori_loop(1, NS, send_rows, 0)
    big[pl.ds(me, 1), pl.ds(pl.multiple_of(T + s * CAP, 16), CAP), :] = dsp[
        pl.ds(pl.multiple_of(s * CAP, 16), CAP), :
    ].reshape(1, CAP, T)

    def span(i):
        return pl.ds(0, T) if i == 0 else pl.ds(T + (i - 1) * RC, RC)

    flows = ((NA, sign, ring_a), (NB, -sign, ring_b))
    CH = NCH + 1

    def to_peer(j, i):
        ref = big.at[j, span(i)]
        rcopy(ref, ref, send.at[6], peer_sem.at[j // 2, i], partner).start()

    def to_ring(flow, j, k, i):
        n, sg, sems = flows[flow]
        ref = big.at[j, span(i)]
        rcopy(ref, ref, send.at[6], sems.at[k, i], (s, chip(sg) * 2 + c)).start()

    def begin(i):
        to_ring(0, me, 0, i)
        to_ring(1, me, 0, i)
        to_peer(me, i)

    def hop(k, i):
        for flow in (0, 1):
            n, sg, sems = flows[flow]
            if k <= n:
                j = chip(-sg * k) * 2 + c
                arrived(big.at[j, span(i)], sems.at[k - 1, i])
                if k < n:
                    to_ring(flow, j, k, i)
                to_peer(j, i)

    def take(ref, o, part_rows):
        a = ref[pl.ds(2 * o, 1), part_rows, :].reshape(-1, T).astype(F32)
        b = ref[pl.ds(2 * o + 1, 1), part_rows, :].reshape(-1, T).astype(F32)
        ga = gn[pl.ds(2 * o, 1), :, :].reshape(1, T)
        gb = gn[pl.ds(2 * o + 1, 1), :, :].reshape(1, T)
        both = jnp.concatenate([(a * ga).astype(BF16), (b * gb).astype(BF16)], axis=1)
        return both, a * a + b * b

    def cols(o):
        return pl.ds(pl.multiple_of(o * 2 * T, 2 * T), 2 * T)

    def add_to(ref, value, first):
        ref[...] = value if first else ref[...] + value

    def routed_in(o, first=False):
        for i in range(1, CH):
            ref = big.at[2 * o + 1 - c, span(i)]
            arrived(ref, peer_sem.at[o, i])
        both, squares = take(big, o, slice(T, T + R))
        add_to(ssq, squares, first)
        add_to(accg, dot(both, eg[cols(o), :]), first)
        add_to(accu, dot(both, eu[cols(o), :]), first)

    def shared_in(o, first=False):
        arrived(big.at[2 * o + 1 - c, span(0)], peer_sem.at[o, 0])
        both, squares = take(big, o, slice(0, T))
        add_to(sss, squares, first)
        add_to(accs, dot_nt(both, sgu[:, cols(o)]), first)

    begin(0)
    early = min(2, NA)
    for k in range(1, early + 1):
        hop(k, 0)
    arrived(gn.at[pl.ds(0, NT - 1)], gn_sem.at[0])
    for i in range(1, CH):

        def wait_rows(q, _, i=i):
            b = (i - 1) * BPC + q

            @pl.when(b != s)
            def _():
                arrived(block_rows(big.at[me], b, T), disp_sem.at[b])

            return 0

        lax.fori_loop(0, BPC, wait_rows, 0)
        begin(i)
    for k in range(early + 1, NA + 1):
        hop(k, 0)
    for load in loads[1:]:
        load.wait()
    shared_in(y, True)
    for off in range(1, Y):
        shared_in(chip(off))
    model_scale = 1.0 / D
    rs_s = lax.rsqrt(jnp.sum(sss[...], axis=1, keepdims=True) * model_scale + 1e-6)
    sh = accs[...] * rs_s
    sh_hidden = (silu(sh) * pltpu.roll(sh, 64, 1))[:, 0:64].astype(BF16)
    for k in range(1, NA + 1):
        for i in range(1, CH):
            hop(k, i)
        if k == 1:
            routed_in(y, True)
        else:
            routed_in(chip(k - 1))
            routed_in(chip(1 - k))
    if NB == NA - 1:
        routed_in(chip(NA))
    rs_r = lax.rsqrt(jnp.sum(ssq[...], axis=1, keepdims=True) * model_scale + 1e-6)
    hidden = (silu(accg[...] * rs_r) * (accu[...] * rs_r)).astype(BF16)

    def down(o):
        v = dot(hidden, ed[:, cols(o)]).astype(BF16)
        part[pl.ds(2 * o, 1), T : T + R, :] = v[:, 0:T].reshape(1, R, T)
        part[pl.ds(2 * o + 1, 1), T : T + R, :] = v[:, T : 2 * T].reshape(1, R, T)
        give(o, pl.ds(T, R), 0)

    def shared_down(o):
        v = dot(sh_hidden, sd[:, cols(o)]).astype(BF16)
        part[pl.ds(2 * o, 1), 0:T, :] = v[:, 0:T].reshape(1, T, T)
        part[pl.ds(2 * o + 1, 1), 0:T, :] = v[:, T : 2 * T].reshape(1, T, T)
        give(o, pl.ds(0, T), 1)

    def give(o, where, k):
        rcopy(
            part.at[2 * o + 1 - c, where], qbuf.at[o, where], send.at[7], q_sem.at[o, k], partner
        ).start()

    def pair_sum(o, i):
        where = span(i)
        if i == 0:
            arrived(qbuf.at[o, pl.ds(0, T)], q_sem.at[o, 1])
        elif i == 1:
            arrived(qbuf.at[o, pl.ds(T, R)], q_sem.at[o, 0])
        mine = part[pl.ds(2 * o + c, 1), where, :].astype(F32)
        return mine[0] + qbuf[pl.ds(o, 1), where, :].astype(F32)[0]

    rings = ((NA, sign, rs_a, ra, sa), (NB, -sign, rs_b, rb, sb))

    def rs_step(flow, j, i):
        n, sg, sems, got, out = rings[flow]
        if j > n:
            return
        where = span(i)
        value = pair_sum(chip(sg * (n - j + 1)), i)
        if j > 1:
            arrived(got.at[j - 2, where], sems.at[j - 2, i])
            value = value + got[j - 2, where, :].astype(F32)
        out[j - 1, where, :] = value.astype(BF16)
        rcopy(
            out.at[j - 1, where], got.at[j - 1, where], send.at[8], sems.at[j - 1, i],
            (s, chip(sg) * 2 + c),
        ).start()

    def rs_end(i):
        where = span(i)
        value = pair_sum(y, i)
        for n, sg, sems, got, out in rings:
            arrived(got.at[n - 1, where], sems.at[n - 1, i])
            value = value + got[n - 1, where, :].astype(F32)
        fin[where, :] = value.astype(BF16)

    def send_back(q, _):
        @pl.when(q != s)
        def _():
            rcopy(
                block_rows(fin, q, T), block_rows(back, s), send.at[9], back_sem.at[0], (q, me)
            ).start()

        return 0

    order = sorted(range(Y), key=lambda o: -min(o, Y - o))
    for off in order[:3]:
        down(chip(off))
    for i in range(1, CH):
        rs_step(0, 1, i)
        rs_step(1, 1, i)
    for off in order[3:]:
        down(chip(off))
    for o in range(Y):
        shared_down(chip(o))
    for j in range(2, NA + 1):
        for i in range(1, CH):
            rs_step(0, j, i)
            rs_step(1, j, i)
    rs_step(0, 1, 0)
    rs_step(1, 1, 0)
    for i in range(1, CH):
        rs_end(i)
        lax.fori_loop((i - 1) * BPC, i * BPC, send_back, 0)
    back[pl.ds(pl.multiple_of(s * CAP, 16), CAP), :] = fin[
        pl.ds(pl.multiple_of(T + s * CAP, 16), CAP), :
    ]
    for j in range(2, NA + 1):
        rs_step(0, j, 0)
        rs_step(1, j, 0)
    rs_end(0)

    arrived(back.at[pl.ds(0, R - CAP)], back_sem.at[0])
    result = hbuf[...] + fin[0:T, :].astype(F32)
    for k in range(2):
        slot_cols = as_columns(slot_scr[k : k + 1, :], T)
        picks = jnp.concatenate(
            [
                ones_where(slot_cols == (la_i + q * T).astype(F32)).astype(BF16)
                for q in range(R // T)
            ],
            axis=1,
        )
        result = result + as_columns(weights_ref[k : k + 1, :], T) * dot(picks, back[...])
    out_ref[...] = result.astype(BF16)

    sent(cb.at[pl.ds(0, NS - 1)], 0)
    sent(wq.at[pl.ds(0, NT - 1)], 1)
    sent(gn.at[pl.ds(0, NT - 1)], 2)
    sent(xprev, 3)
    sent(pk.at[pl.ds(0, NT - 1)], 4)
    sent(dsp.at[pl.ds(0, R - CAP)], 5)
    sent(big.at[pl.ds(0, NT - 1)], 6)
    sent(qbuf, 7)
    sent(qbuf.at[pl.ds(0, Y - 1)], 8)
    sent(back.at[pl.ds(0, R - CAP)], 9)


def layer(cfg, *args):
    (pool_input, doc_ids, residual, pool_gain, out_proj, norm_gain, routes, route_weights,
     expert_gate, expert_up, expert_down, shared_gate, shared_up, shared_down) = args
    NS, NT, T, CAP, NCH = cfg
    Y = NT // 2
    R = NS * CAP
    NA, NB = Y // 2, Y - 1 - Y // 2
    CH = NCH + 1
    D = NT * T
    E = T + R
    FH = expert_gate.shape[2]
    inputs = (
        pool_input.T, doc_ids.reshape(1, T), residual, pool_gain.reshape(1, -1),
        norm_gain.reshape(1, T), routes.T, route_weights.T,
        out_proj, expert_gate, expert_up, expert_down, shared_gate.T, shared_up.T, shared_down,
    )
    vm = pl.BlockSpec(memory_space=pltpu.VMEM)
    hbm = pl.BlockSpec(memory_space=pl.ANY)
    scratch = [
        VMEM((64, D), BF16), VMEM((D, FH), BF16), VMEM((D, FH), BF16), VMEM((FH, D), BF16),
        VMEM((128, D), BF16), VMEM((64, D), BF16), DMA((7,)),
        VMEM((NS, 1, T), F32), VMEM((64, T), BF16), VMEM((NT, 64, T), BF16),
        VMEM((NT, 1, T), F32), VMEM((NT, 64, T), BF16), VMEM((R, T), BF16),
        VMEM((NT, E, T), BF16), VMEM((NT, E, T), BF16), VMEM((Y, E, T), BF16),
        VMEM((NA, E, T), BF16), VMEM((NB, E, T), BF16), VMEM((NA, E, T), BF16),
        VMEM((NB, E, T), BF16), VMEM((E, T), BF16), VMEM((R, T), BF16),
        VMEM((1, T), F32), VMEM((T, T), F32), VMEM((R, FH), F32), VMEM((R, FH), F32),
        VMEM((R, T), F32), VMEM((T, 128), F32), VMEM((T, T), F32), VMEM((8, T), F32),
        DMA((10,)), DMA((1,)), DMA((1,)), DMA((1,)), DMA((1,)), DMA((NT,)), DMA((NS,)),
        DMA((NA, CH)), DMA((NB, CH)), DMA((Y, CH)), DMA((Y, 2)), DMA((NA, CH)), DMA((NB, CH)),
        DMA((1,)),
    ]
    return pl.pallas_call(
        functools.partial(kernel, cfg),
        out_shape=jax.ShapeDtypeStruct((T, T), BF16),
        in_specs=[vm] * 7 + [hbm] * 7,
        out_specs=vm,
        scratch_shapes=scratch,
        compiler_params=pltpu.CompilerParams(
            collective_id=0, has_side_effects=True, vmem_limit_bytes=67043328
        ),
    )(*inputs)


def solution(mesh, cap=None):
    NS, NT = mesh.shape["sp"], mesh.shape["tp"]
    placed = (
        P("sp", "tp"), P("sp"), P("sp", "tp"), P("tp"), P("tp", None), P("tp"), P("sp", None),
        P("sp", None), P("sp", None, "tp"), P("sp", None, "tp"), P("sp", "tp", None),
        P(None, "tp"), P(None, "tp"), P("tp", None),
    )

    def body(*args):
        T = args[1].shape[0]
        top = args[6].shape[1]
        most = cap or 16 * max(1, 2 * T * top // (NS * 16))
        return layer((NS, NT, T, most, min(4, NS)), *args)

    return jax.shard_map(body, mesh=mesh, in_specs=placed, out_specs=P("sp", "tp"), check_vma=False)
```

time: 280 us -> 85.3 us (0.30)
  the two profiles are of different devices: /device:TPU:1 before, /device:TPU:8 now
where the time goes in v1:
time: 85.3 us; the launch traced here: 85 us
  Pallas kernels  83.6 us (98%)
  local copies, waits for them, and re-layouts  1.38 us (2%)
    pallas_call x1, Pallas kernels, layer(): pl.pallas_call(functools.partial(kernel, cfg), out_shape=jax.ShapeDtypeSt...  83.6 us

profile of v1, /device:TPU:8, one launch (start us, length us, event | category | flops | bytes accessed | tf_op | source)
XLA Modules:
  0.0 85.0 jit_solution(13170118202962456185)
XLA Ops:
  0.0 83.6 %shard_map.136 = bf16[128,128]{1,0:T(8,128)(2,1)} custom-call(bf16[64,128]{1,0:T(8,128)(2,1)} %bitcast.10, s32[1,128]{1,0:T(1,128)} %bitcast.13, bf16[128,128]{1,0:T(8,128)(2,1)} %residual_ref.1, f32[1,64]{1,0:T(1,128)} %bitcast.14, f32[1,128]{1,0:T(1,128)} %bitcast.15, s32[2,128]{1,0:T(2,128)} %bitcast.11, f32[2,128]{1,0:T(2,128)} %bitcast.12, ...), custom_call_target="tpu_custom_call" | custom-call | tf_op jit(solution)/shard_map/pallas_call | solution.py:485
  83.7 1.4 %copy.16 = bf16[128,128]{1,0:T(8,128)(2,1)} copy(bf16[128,128]{1,0:T(8,128)(2,1)} %shard_map.136) | data formatting | bytes 65536
